TPU v7x, 32 devices: a whole 2x2x4 slice. The times are simulated.
32 devices in a mesh: ep: 4 (over y, x), tp: 8 (over z, core).
Axes of the slice: x: 2, y: 2, z: 4, core: 2. Of those that a mesh axis runs over, the one named last changes fastest.
Arguments:
- pool_in: bfloat16 [16384, 1024], P(('ep', 'tp')), may hold values from -6 to 6
- pool_weight: bfloat16 [4, 256, 256], replicated, may hold values from -0.375 to 0.375
- pool_gain: float32 [1024], replicated, may hold values from 0.1 to 1.9
- out_weight: bfloat16 [1024, 2048], P('tp'), may hold values from -0.1875 to 0.1875
- mix_gain: float32 [2048], replicated, may hold values from 0.1 to 1.9
- expert_in: bfloat16 [1024, 2048], P('ep'), may hold values from -6 to 6
- routes: int32 [1024, 4], P('ep'), may hold values from 0 to 7, all different within a row; in each aligned block of 32 rows (0 to 31, 32 to 63, ...) at most 32 rows name the same one
- route_weight: float32 [1024, 4], P('ep'), may hold values from 0.1 to 1
- pre_gain: float32 [2048], replicated, may hold values from 0.1 to 1.9
- gate_weight: bfloat16 [8, 2048, 4096], P('ep', None, 'tp'), may hold values from -0.39648438 to 0.39648438
- up_weight: bfloat16 [8, 2048, 4096], P('ep', None, 'tp'), may hold values from -0.39648438 to 0.39648438
- down_weight: bfloat16 [8, 4096, 2048], P('ep', 'tp'), may hold values from -0.09375 to 0.09375
- post_gain: float32 [2048], replicated, may hold values from 0.1 to 1.9
Outputs:
- mix_out: bfloat16 [16384, 2048], P(('ep', 'tp'))
- expert_out: bfloat16 [1024, 2048], P(('ep', 'tp'))
Inputs may be any that keep to these rules, and one draw needn't show every extreme that they name: `routes`: each row names 4 different experts. In each aligned block of 32 rows no expert is named by more than 32 rows, a bound that some block reaches.
All inputs are finite; a program needn't handle non-finite values.
Results may differ from a plain program's by a relative error of at most 0.019.
Values may be sent and summed in bfloat16 or wider, within the bound.
A program may use at most 128 MiB of HBM per device.

v0:
```python
import jax
import jax.numpy as jnp
from jax import lax
from jax.sharding import PartitionSpec as P

WINDOWS = (2, 4, 8, 16)
EPS = 1e-06
LIMIT = 7.0
ALPHA = 1.702


def shifted(block, axis, distance):
    devices = range(lax.axis_size(axis))
    route = [(i - distance, i) for i in devices if i - distance in devices]
    return lax.ppermute(block, axis, route)


def rms_scale(values, gain):
    mean_square = jnp.mean(values * values, axis=-1, keepdims=True)
    return values * lax.rsqrt(mean_square + EPS) * gain


def trailing_pool(padded, first_pos, rows):
    group = padded.shape[1] // 4
    position = first_pos + jnp.arange(rows, dtype=jnp.int32)
    pieces = []
    for which, window in enumerate(WINDOWS):
        channels = padded[:, which * group : (which + 1) * group]
        running = channels[16 : 16 + rows]
        for reach in range(2, window + 1):
            running = running + channels[17 - reach : 17 - reach + rows]
        count = jnp.minimum(position + 1, window).astype(jnp.float32)[:, None]
        pieces.append(running / count)
    pooled = jnp.concatenate(pieces, axis=1)
    return (pooled - padded[16:]).astype(jnp.bfloat16)


def selection(block_routes, experts, capacity):
    flat = block_routes.reshape(-1)
    onehot = (flat[:, None] == jnp.arange(experts, dtype=jnp.int32)[None, :]).astype(jnp.int32)
    earlier = jnp.cumsum(onehot, axis=0) - onehot
    rank = jnp.sum(earlier * onehot, axis=1)
    slots = (flat * capacity + rank).reshape(block_routes.shape)
    return (
        slots[:, :, None] == jnp.arange(experts * capacity, dtype=jnp.int32)[None, None, :]
    ).astype(jnp.bfloat16)


def clamped_unit(gate, up):
    gate = jnp.minimum(gate, LIMIT)
    up = jnp.clip(up, -LIMIT, LIMIT)
    return (up + 1.0) * gate * jax.nn.sigmoid(ALPHA * gate)


def hidden_rows(arrived, gate_weight, up_weight):
    gate = jnp.einsum("necd,edf->necf", arrived, gate_weight, preferred_element_type=jnp.float32)
    up = jnp.einsum("necd,edf->necf", arrived, up_weight, preferred_element_type=jnp.float32)
    return clamped_unit(gate, up).astype(jnp.bfloat16)


def body(
    pool_in,
    pool_weight,
    pool_gain,
    out_weight,
    mix_gain,
    expert_in,
    routes,
    route_weight,
    pre_gain,
    gate_weight,
    up_weight,
    down_weight,
    post_gain,
):
    rows, channels = pool_in.shape
    width = out_weight.shape[1]
    rim = shifted(pool_in[rows - 16 :], ("ep", "tp"), 1)
    padded = jnp.concatenate([rim, pool_in], axis=0).astype(jnp.float32)
    first_pos = (lax.axis_index("ep") * lax.axis_size("tp") + lax.axis_index("tp")) * rows
    diff = trailing_pool(padded, first_pos, rows)
    mixed = jnp.einsum(
        "sgc,gcd->sgd",
        diff.reshape(rows, 4, channels // 4),
        pool_weight,
        preferred_element_type=jnp.float32,
    )
    mixed = (mixed.reshape(rows, channels) * pool_gain).astype(jnp.bfloat16)
    projected = jnp.dot(
        mixed,
        lax.all_gather(out_weight, "tp", axis=0, tiled=True),
        preferred_element_type=jnp.float32,
    )
    mix_out = rms_scale(projected, mix_gain).astype(jnp.bfloat16)
    ep_count = lax.axis_size("ep")
    tp_count = lax.axis_size("tp")
    tp_place = lax.axis_index("tp")
    local_experts = gate_weight.shape[0]
    experts = local_experts * ep_count
    tokens_here, choose = routes.shape
    block_tokens = tokens_here // tp_count
    capacity = 2 * block_tokens * choose // experts
    block_routes = lax.dynamic_slice_in_dim(routes, tp_place * block_tokens, block_tokens, 0)
    block_rows = lax.dynamic_slice_in_dim(expert_in, tp_place * block_tokens, block_tokens, 0)
    normed = rms_scale(block_rows.astype(jnp.float32), pre_gain).astype(jnp.bfloat16)
    own_picks = selection(block_routes, experts, capacity)
    buffer = jnp.einsum(
        "ts,td->sd", jnp.sum(own_picks, axis=1), normed, preferred_element_type=jnp.float32
    ).astype(jnp.bfloat16)
    buffer = buffer.reshape(ep_count, local_experts, capacity, width)
    arrived = lax.all_to_all(buffer, "ep", split_axis=0, concat_axis=0, tiled=True)
    hidden_all = hidden_rows(
        lax.all_gather(arrived, "tp", axis=0, tiled=True), gate_weight, up_weight
    )
    summed = lax.psum_scatter(
        jnp.einsum(
            "necf,efd->necd", hidden_all, down_weight, preferred_element_type=jnp.float32
        ).astype(jnp.bfloat16),
        "tp",
        scatter_dimension=0,
        tiled=True,
    )
    returned = lax.all_to_all(summed, "ep", split_axis=0, concat_axis=0, tiled=True)
    returned = returned.reshape(experts * capacity, width)
    per_route = jnp.einsum("tks,sd->tkd", own_picks, returned, preferred_element_type=jnp.float32)
    weights = lax.dynamic_slice_in_dim(route_weight, tp_place * block_tokens, block_tokens, 0)
    combined = jnp.sum(per_route * weights[:, :, None], axis=1)
    expert_out = rms_scale(combined, post_gain).astype(jnp.bfloat16)
    return (mix_out, expert_out)


def solution(mesh):
    return jax.shard_map(
        body,
        mesh=mesh,
        in_specs=(
            P(("ep", "tp"), None),
            P(),
            P(),
            P("tp", None),
            P(),
            P("ep", None),
            P("ep", None),
            P("ep", None),
            P(),
            P("ep", None, "tp"),
            P("ep", None, "tp"),
            P("ep", "tp", None),
            P(),
        ),
        out_specs=(P(("ep", "tp"), None), P(("ep", "tp"), None)),
        check_vma=False,
    )
```

profile of v0, /device:TPU:0, one launch (start us, length us, event | category | flops | bytes accessed | tf_op | source)
XLA Modules:
  0.0 364.8 jit_solution(16986653693718660319)
XLA Ops:
  7.2 0.0 copy-start
  7.2 0.0 all-gather.5.cloned.1.call-start
  7.2 0.8 constant_dynamic-slice_fusion.1
  8.0 0.1 copy.38
  8.1 0.1 eq.28
  8.2 0.1 fusion.36
  8.3 0.2 reduce_window_sum.11
  8.5 0.2 select_reduce_fusion
  8.7 0.1 reduce_sum.61
  8.8 0.1 copy.29
  8.9 0.1 fusion.34
  9.0 1.0 fusion.26
  10.0 1.4 convolution_convert_fusion
  11.5 19.1 %all_to_all.10 = bf16[4,2,32,2048]{3,2,1,0:T(8,128)(2,1)S(1)} all-to-all(bf16[4,2,32,2048]{3,2,1,0:T(8,128)(2,1)S(1)} %bitcast.56), channel_id=1, replica_groups=mesh['ep'=4,'tp'=8] {'ep'}, dimensions={0} | all-to-all | bytes 2097152 | tf_op jit(solution)/shard_map/all_to_all | solution.py:111
  30.6 1.0 copy.30
  31.6 0.0 all-gather.5.cloned.1.call-update
  31.6 0.0 all-gather.3.cloned.1.call-start
  31.7 0.7 all-gather.3.cloned.1.call-update
  32.4 0.0 all-reduce.3.cloned.1.call-start
  32.4 81.1 %all-gather.5.cloned.1.call-done = bf16[32,2,32,2048]{3,2,0,1:T(8,128)(2,1)} async-done(((bf16[4,2,32,2048]{3,2,0,1:T(8,128)(2,1)}), bf16[32,2,32,2048]{3,2,0,1:T(8,128)(2,1)}) %all-gather.5.cloned.1.call-update) | async-done | bytes 8388624 | tf_op jit(solution)/shard_map/all_gather | solution.py:113
  113.6 11.0 %fusion.3 = f32[2,32,32,512]{3,2,1,0:T(8,128)} fusion(bf16[32,2,32,2048]{3,2,0,1:T(8,128)(2,1)} %all-gather.5.cloned.1.call-done, bf16[2,2048,512]{2,1,0:T(8,128)(2,1)} %param.23), kind=kOutput, calls=%fused_computation.4 | convolution fusion | flops 4294967296 | bytes 16777216 | tf_op jit(solution)/shard_map/necd,edf->necf/dot_general | solution.py:57
  124.6 15.9 %convert_bitcast_fusion = bf16[32,2,32,2048]{3,2,0,1:T(8,128)(2,1)} fusion(bf16[2,512,2048]{2,1,0:T(8,128)(2,1)} %param.24, f32[2,32,32,512]{3,2,1,0:T(8,128)} %fusion.3, bf16[32,2,32,2048]{3,2,0,1:T(8,128)(2,1)} %all-gather.5.cloned.1.call-done, bf16[2,2048,512]{2,1,0:T(8,128)(2,1)} %param.22), kind=kOutput, calls=%fused_computation | convolution fusion | flops 8604614656 | bytes 29360128 | tf_op jit(solution)/shard_map/necf,efd->necd/dot_general | solution.py:116
  140.5 0.0 copy-start.1
  140.5 0.0 copy-start.5
  140.5 0.0 copy-start.6
  140.5 0.0 all-reduce.3.cloned.1.call-update
  140.5 1.2 copy-done.1
  141.7 2.3 collective-permute-start
  144.1 0.0 copy-done.5
  144.1 0.1 constant_dynamic-slice_fusion
  144.2 0.0 copy-done.6
  144.2 0.6 dynamic-slice
  145.4 0.0 collective-permute-done
  145.4 0.3 maximum_convert_fusion
  145.7 0.6 fusion.22
  146.3 0.6 fusion.25
  147.0 0.0 copy-start.4
  147.0 0.4 fusion.7
  147.5 0.0 copy-done
  147.5 0.5 fusion.19
  148.0 0.0 copy-done.4
  148.0 0.2 fusion.8
  148.2 12.7 %all-gather.3.cloned.1.call-done = bf16[1024,2048]{1,0:T(8,128)(2,1)} async-done(((bf16[128,2048]{1,0:T(8,128)(2,1)}), bf16[1024,2048]{1,0:T(8,128)(2,1)}) %all-gather.3.cloned.1.call-update) | async-done | bytes 4194320 | tf_op jit(solution)/shard_map/all_gather | solution.py:91
  160.9 6.6 %multiply_reduce_fusion = (f32[512]{0:T(512)S(1)}, f32[512,2048]{1,0:T(8,128)}) fusion(bf16[512,1024]{0,1:T(8,128)(2,1)S(1)} %fusion.8, bf16[1024,2048]{1,0:T(8,128)(2,1)} %all-gather.3.cloned.1.call-done), kind=kOutput, calls=%fused_computation.8 | convolution fusion | flops 2149580288 | bytes 9439232 | tf_op jit(solution)/shard_map/dot_general | solution.py:89
  167.5 0.0 copy-start.2
  167.5 170.1 %all-reduce.3.cloned.1.call-done = bf16[32,2,32,2048]{3,2,0,1:T(8,128)(2,1)} async-done(((bf16[32,2,32,2048]{3,2,0,1:T(8,128)(2,1)}), bf16[32,2,32,2048]{3,2,0,1:T(8,128)(2,1)}) %all-reduce.3.cloned.1.call-update) | async-done | bytes 8388624
  337.6 1.3 constant_dynamic-slice_fusion.2
  338.9 1.1 copy.31
  339.9 3.6 all-to-all-start.1
  343.6 0.0 copy-start.3
  343.6 0.0 copy-done.2
  343.6 3.9 %multiply_convert_fusion.1 = bf16[512,2048]{1,0:T(8,128)(2,1)} fusion(f32[512,2048]{1,0:T(8,128)} %get-tuple-element.6, f32[2048]{0:T(1024)S(1)} %copy-done.2, f32[512]{0:T(512)S(1)} %add_rsqrt_fusion), kind=kLoop, calls=%fused_computation.7 | loop fusion | flops 3145728 | bytes 6301696 | tf_op jit(solution)/shard_map/convert_element_type | solution.py:94
  347.5 9.5 %all-to-all-done.1 = bf16[4,2,32,2048]{3,2,1,0:T(8,128)(2,1)S(1)} async-done(((bf16[4,2,32,2048]{3,2,1,0:T(8,128)(2,1)}), bf16[4,2,32,2048]{3,2,1,0:T(8,128)(2,1)S(1)}, u32[]{:S(2)}, u32[]{:S(2)}) %all-to-all-start.1) | async-done | bytes 1048608 | tf_op jit(solution)/shard_map/all_to_all | solution.py:123
  357.0 0.3 fusion.18
  357.4 0.1 multiply_reduce_fusion.1
  357.5 0.0 copy-done.3
  357.5 0.8 multiply_convert_fusion.2
  (7 shorter events, 0.0 us)
Async XLA Ops:
  7.2 140.3 %copy-start = (bf16[4,256,256]{2,1,0:T(8,128)(2,1)S(1)}, bf16[4,256,256]{2,1,0:T(8,128)(2,1)}, u32[]{:S(2)}) copy-start(bf16[4,256,256]{2,1,0:T(8,128)(2,1)} %param.14) | copy-start | bytes 1572868
  7.2 106.4 %all-gather.5.cloned.1.call-start = ((), (), s32[]{:S(2)}) async-start(), calls=%async_computation.3 | async-start | bytes 9437184 | tf_op jit(solution)/shard_map/all_gather | solution.py:113
  31.6 129.2 %all-gather.3.cloned.1.call-start = ((), (), s32[]{:S(2)}) async-start(), calls=%async_computation.2 | async-start | bytes 4718592 | tf_op jit(solution)/shard_map/all_gather | solution.py:91
  32.4 305.2 %all-reduce.3.cloned.1.call-start = ((), (), s32[]{:S(2)}) async-start(), calls=%async_computation.4 | async-start | bytes 16777216
  140.5 1.2 copy-start.1
  140.5 3.6 copy-start.5
  140.5 3.7 %copy-start.6 = (u32[32]{0:T(128)S(1)}, u32[32]{0:T(128)}, u32[]{:S(2)}) copy-start(u32[32]{0:T(128)} %constant.59) | copy-start | bytes 388
  141.7 3.7 %collective-permute-start = (bf16[16,1024]{1,0:T(8,128)(2,1)S(1)}, bf16[16,1024]{1,0:T(8,128)(2,1)S(1)}, u32[]{:S(2)}, u32[]{:S(2)}) collective-permute-start(bf16[16,1024]{1,0:T(8,128)(2,1)S(1)} %slice.130), channel_id=1, source_target_pairs={{0,1},{1,2},{2,3},{3,4},{4,5},{5,6},{6,7},{7,8},{8,9},{9,10},{10,1... | collective-permute-start | bytes 98312 | tf_op jit(solution)/shard_map/ppermute | solution.py:15
  147.0 1.0 copy-start.4
  167.5 176.1 %copy-start.2 = (f32[2048]{0:T(1024)S(1)}, f32[2048]{0:T(1024)}, u32[]{:S(2)}) copy-start(f32[2048]{0:T(1024)} %param.17) | copy-start | bytes 24580
  339.9 17.1 %all-to-all-start.1 = ((bf16[4,2,32,2048]{3,2,1,0:T(8,128)(2,1)}), bf16[4,2,32,2048]{3,2,1,0:T(8,128)(2,1)S(1)}, u32[]{:S(2)}, u32[]{:S(2)}) async-start(bf16[4,2,32,2048]{3,2,1,0:T(8,128)(2,1)} %copy.31), calls=%async_computation.1 | async-start | bytes 2097152 | tf_op jit(solution)/shard_map/all_to_all | solution.py:123
  343.6 13.9 %copy-start.3 = (f32[2048]{0:T(1024)S(1)}, f32[2048]{0:T(1024)}, u32[]{:S(2)}) copy-start(f32[2048]{0:T(1024)} %param.25) | copy-start | bytes 24580
Sparse Core Ops, SparseCore 0:
  31.8 81.7 all-gather.4
  115.1 45.6 all-gather.2
  163.3 174.2 all-reduce.2
where the time goes:
time: 365 us
  waiting for transfers between devices  274 us (75%)
  matrix products  35.8 us (10%)
  blocking collectives  19.1 us (5%)
  between operations  14.6 us (4%)
  other arithmetic  8.59 us (2%)
  local copies, waits for them, and re-layouts  6.46 us (2%)
  starting transfers between devices  6.08 us (2%)
    unnamed x4, waiting for transfers between devices  171 us
    all_gather x1, waiting for transfers between devices, body(): lax.all_gather(arrived, 'tp', axis=0, tiled=True)  81.1 us
    all_to_all x1, blocking collectives, body(): lax.all_to_all(buffer, 'ep', split_axis=0, concat_axis=0, tiled=True)  19.1 us
    dot_general x1, matrix products, body(): jnp.einsum('necf,efd->necd', hidden_all, down_weight, preferred_element_t...  15.9 us
    all_gather x1, waiting for transfers between devices, body(): lax.all_gather(out_weight, 'tp', axis=0, tiled=True)  12.7 us
    dot_general x1, matrix products, hidden_rows(): jnp.einsum('necd,edf->necf', arrived, up_weight, preferred_element_type=j...  11 us
    all_to_all x1, waiting for transfers between devices, body(): lax.all_to_all(summed, 'ep', split_axis=0, concat_axis=0, tiled=True)  9.5 us
  transfers between devices with their start and end apart: 5, of which 4 were waited for; matrix products, arithmetic and copies ran while one was open for 11% of the time, Pallas kernels for 0%

commit v1 on v0

v1 whole, which is shorter than its diff:
```python
import jax
import jax.numpy as jnp
from jax import lax
from jax.sharding import PartitionSpec as P

WINDOWS = (2, 4, 8, 16)
EPS = 1e-06
LIMIT = 7.0
ALPHA = 1.702


def shifted(block, axis, distance):
    devices = range(lax.axis_size(axis))
    route = [(i - distance, i) for i in devices if i - distance in devices]
    return lax.ppermute(block, axis, route)


def rms_scale(values, gain):
    mean_square = jnp.mean(values * values, axis=-1, keepdims=True)
    return values * lax.rsqrt(mean_square + EPS) * gain


def trailing_pool(padded, first_pos, rows):
    group = padded.shape[1] // 4
    position = first_pos + jnp.arange(rows, dtype=jnp.int32)
    pieces = []
    for which, window in enumerate(WINDOWS):
        channels = padded[:, which * group : (which + 1) * group]
        running = channels[16 : 16 + rows]
        for reach in range(2, window + 1):
            running = running + channels[17 - reach : 17 - reach + rows]
        count = jnp.minimum(position + 1, window).astype(jnp.float32)[:, None]
        pieces.append(running / count)
    pooled = jnp.concatenate(pieces, axis=1)
    return (pooled - padded[16:]).astype(jnp.bfloat16)


def expert_weights(routes, route_weight, experts):
    chosen = routes[:, :, None] == jnp.arange(experts, dtype=jnp.int32)[None, None, :]
    return jnp.sum(jnp.where(chosen, route_weight[:, :, None], 0.0), axis=1)


def clamped_unit(gate, up):
    gate = jnp.minimum(gate, LIMIT)
    up = jnp.clip(up, -LIMIT, LIMIT)
    return (up + 1.0) * gate * jax.nn.sigmoid(ALPHA * gate)


def body(
    pool_in,
    pool_weight,
    pool_gain,
    out_weight,
    mix_gain,
    expert_in,
    routes,
    route_weight,
    pre_gain,
    gate_weight,
    up_weight,
    down_weight,
    post_gain,
):
    rows, channels = pool_in.shape
    width = out_weight.shape[1]
    rim = shifted(pool_in[rows - 16 :], ("ep", "tp"), 1)
    padded = jnp.concatenate([rim, pool_in], axis=0).astype(jnp.float32)
    first_pos = (lax.axis_index("ep") * lax.axis_size("tp") + lax.axis_index("tp")) * rows
    diff = trailing_pool(padded, first_pos, rows)
    mixed = jnp.einsum(
        "sgc,gcd->sgd",
        diff.reshape(rows, 4, channels // 4),
        pool_weight,
        preferred_element_type=jnp.float32,
    )
    mixed = (mixed.reshape(rows, channels) * pool_gain).astype(jnp.bfloat16)
    projected = jnp.dot(
        mixed,
        lax.all_gather(out_weight, "tp", axis=0, tiled=True),
        preferred_element_type=jnp.float32,
    )
    mix_out = rms_scale(projected, mix_gain).astype(jnp.bfloat16)
    ep_place = lax.axis_index("ep")
    local_experts = gate_weight.shape[0]
    experts = local_experts * lax.axis_size("ep")
    weights = expert_weights(routes, route_weight, experts)
    weights = lax.all_gather(weights, "ep", axis=0, tiled=True)
    weights = lax.dynamic_slice_in_dim(weights, ep_place * local_experts, local_experts, 1)
    normed = rms_scale(expert_in.astype(jnp.float32), pre_gain).astype(jnp.bfloat16)
    normed = lax.all_gather(normed, "ep", axis=0, tiled=True)
    hidden = []
    for which in range(local_experts):
        gate = jnp.dot(normed, gate_weight[which], preferred_element_type=jnp.float32)
        up = jnp.dot(normed, up_weight[which], preferred_element_type=jnp.float32)
        hidden.append(
            (clamped_unit(gate, up) * weights[:, which : which + 1]).astype(jnp.bfloat16)
        )
    hidden = jnp.concatenate(hidden, axis=1)
    partial = jnp.dot(
        hidden, down_weight.reshape(-1, width), preferred_element_type=jnp.float32
    ).astype(jnp.bfloat16)
    combined = lax.psum_scatter(
        partial, ("ep", "tp"), scatter_dimension=0, tiled=True
    ).astype(jnp.float32)
    expert_out = rms_scale(combined, post_gain).astype(jnp.bfloat16)
    return (mix_out, expert_out)


def solution(mesh):
    return jax.shard_map(
        body,
        mesh=mesh,
        in_specs=(
            P(("ep", "tp"), None),
            P(),
            P(),
            P("tp", None),
            P(),
            P("ep", None),
            P("ep", None),
            P("ep", None),
            P(),
            P("ep", None, "tp"),
            P("ep", None, "tp"),
            P("ep", "tp", None),
            P(),
        ),
        out_specs=(P(("ep", "tp"), None), P(("ep", "tp"), None)),
        check_vma=False,
    )
```

time: 365 us -> 270 us (0.74)
  waiting for transfers between devices: 274 us -> 207 us
  matrix products: 35.8 us -> 25.4 us
  blocking collectives: 19.1 us -> 9.67 us
  local copies, waits for them, and re-layouts: 6.46 us -> 1.47 us
  starting transfers between devices: 6.08 us -> 1.64 us
    unnamed x4 -> x3, waiting for transfers between devices: 171 us -> 0.73 us
    reduce_scatter x0 -> x1, waiting for transfers between devices: none -> 138 us  [body(): lax.psum_scatter(partial, ('ep', 'tp'), scatter_dimension=0, tiled=True)]
    all_gather x1, waiting for transfers between devices: 81.1 us -> 44.9 us  [body(): normed = lax.all_gather(normed, 'ep', axis=0, tiled=True)]
    all_to_all x1 -> x0, blocking collectives: 19.1 us -> none  [body(): lax.all_to_all(buffer, 'ep', split_axis=0, concat_axis=0, tiled=True)]
    all_gather x0 -> x1, blocking collectives: none -> 9.67 us  [body(): weights = lax.all_gather(weights, 'ep', axis=0, tiled=True)]
    all_to_all x1 -> x0, waiting for transfers between devices: 9.5 us -> none  [body(): lax.all_to_all(summed, 'ep', split_axis=0, concat_axis=0, tiled=True)]
    all_gather x1, waiting for transfers between devices: 12.7 us -> 22 us  [body(): lax.all_gather(out_weight, 'tp', axis=0, tiled=True)]
    dot_general x4 -> x5, matrix products: 28.7 us -> 20.2 us  [the longest x2 7.79 us: body(): up = jnp.dot(normed, up_weight[which], preferred_element_type=jnp.float32)]
  transfers between devices with their start and end apart: 5 -> 4, of which waited for: 4 -> 4; matrix products, arithmetic and copies ran while one was open for 11% -> 11% of each run, Pallas kernels for 0% -> 0%
where the time goes in v1:
time: 270 us
  waiting for transfers between devices  207 us (77%)
  matrix products  25.4 us (9%)
  between operations  14 us (5%)
  other arithmetic  10.7 us (4%)
  blocking collectives  9.67 us (4%)
    reduce_scatter x1, waiting for transfers between devices, body(): lax.psum_scatter(partial, ('ep', 'tp'), scatter_dimension=0, tiled=True)  138 us
    all_gather x1, waiting for transfers between devices, body(): normed = lax.all_gather(normed, 'ep', axis=0, tiled=True)  44.9 us
    all_gather x1, waiting for transfers between devices, body(): lax.all_gather(out_weight, 'tp', axis=0, tiled=True)  22 us
    all_gather x1, blocking collectives, body(): weights = lax.all_gather(weights, 'ep', axis=0, tiled=True)  9.67 us
    dot_general x2, matrix products, body(): up = jnp.dot(normed, up_weight[which], preferred_element_type=jnp.float32)  7.79 us
    dot_general x1, matrix products, body(): jnp.dot(hidden, down_weight.reshape(-1, width), preferred_element_type=jn...  6.47 us
    dot_general x2, matrix products, body(): jnp.dot(normed, gate_weight[which], preferred_element_type=jnp.float32)  5.99 us
  transfers between devices with their start and end apart: 4, of which 4 were waited for; matrix products, arithmetic and copies ran while one was open for 11% of the time, Pallas kernels for 0%

profile of v1, /device:TPU:0, one launch (start us, length us, event | category | flops | bytes accessed | tf_op | source)
XLA Modules:
  0.0 269.7 jit_solution(13656059231238334772)
XLA Ops:
  7.2 0.0 copy-start
  7.2 0.0 all-gather.5.cloned.1.call-start
  7.2 1.6 fusion
  8.8 0.0 copy-start.5
  8.8 0.0 copy-start.6
  8.8 2.5 fusion.2
  11.3 0.0 all-gather.5.cloned.1.call-update
  11.3 0.0 all-gather.3.cloned.1.call-start
  11.4 0.7 all-gather.3.cloned.1.call-update
  12.1 0.0 reduce-scatter.2.cloned.1.call-start
  12.2 0.0 copy-done.5
  12.2 0.0 copy-done.6
  12.2 9.7 %all_gather.11 = f32[1024,8]{0,1:T(8,128)S(1)} all-gather(f32[256,8]{0,1:T(8,128)S(1)} %select_reduce_fusion), channel_id=1, replica_groups=mesh['ep'=4,'tp'=8] {'ep'}, dimensions={0}, use_global_device_ids=true | all-gather | bytes 40960 | tf_op jit(solution)/shard_map/all_gather | solution.py:87
  21.9 44.9 %all-gather.5.cloned.1.call-done = bf16[1024,2048]{1,0:T(8,128)(2,1)} async-done(((bf16[256,2048]{1,0:T(8,128)(2,1)}), bf16[1024,2048]{1,0:T(8,128)(2,1)}) %all-gather.5.cloned.1.call-update) | async-done | bytes 4194320 | tf_op jit(solution)/shard_map/all_gather | solution.py:90
  66.8 0.0 copy-start.7
  66.8 0.0 copy-start.10
  66.8 5.4 %fusion.10 = f32[1024,512]{0,1:T(8,128)S(1)} fusion(bf16[1024,2048]{1,0:T(8,128)(2,1)} %all-gather.5.cloned.1.call-done, bf16[2,2048,512]{2,1,0:T(8,128)(2,1)} %param.23), kind=kOutput, calls=%fused_computation.17 | convolution fusion | flops 2147483648 | bytes 8388608 | tf_op jit(solution)/shard_map/dot_general | solution.py:94
  72.2 0.0 copy-done.7
  72.2 0.0 copy-done.10
  72.2 0.0 copy-start.8
  72.2 2.4 fusion.14
  74.6 0.0 copy-done.8
  74.6 3.0 %multiply_convert_fusion.1 = bf16[1024,512]{0,1:T(8,128)(2,1)S(1)} fusion(f32[1024,512]{0,1:T(8,128)S(1)} %fusion.10, bf16[1024,2048]{1,0:T(8,128)(2,1)S(1)} %copy-done.10, bf16[2,2048,512]{2,1,0:T(8,128)(2,1)S(1)} %copy-done.8, f32[1024]{0:T(1024)S(1)} %bitcast.39), kind=kOutput, calls=%fused_computation.23 | convolution fusion | flops 2153250816 | bytes 9441280 | tf_op jit(solution)/shard_map/dot_general | solution.py:93
  77.6 0.0 copy-start.9
  77.7 3.0 %multiply_convert_fusion.2 = bf16[1024,512]{0,1:T(8,128)(2,1)S(1)} fusion(f32[1024,512]{0,1:T(8,128)S(1)} %fusion.14, bf16[1024,2048]{1,0:T(8,128)(2,1)S(1)} %copy-done.10, bf16[2,2048,512]{2,1,0:T(8,128)(2,1)S(1)} %copy-done.8, f32[1024]{0:T(1024)S(1)} %bitcast.38), kind=kOutput, calls=%fused_computation.26 | convolution fusion | flops 2153250816 | bytes 9441280 | tf_op jit(solution)/shard_map/dot_general | solution.py:93
  80.7 0.0 copy-done.9
  80.7 6.5 %convolution_convert_fusion = bf16[1024,2048]{1,0:T(8,128)(2,1)} fusion(bf16[1024,2048]{1,0:T(8,128)(2,1)S(1)} %bitcast.40, bf16[1024,512]{0,1:T(8,128)(2,1)S(1)} %multiply_convert_fusion.1, bf16[1024,512]{0,1:T(8,128)(2,1)S(1)} %multiply_convert_fusion.2), kind=kOutput, calls=%fused_computation.2 | convolution fusion | flops 4301258752 | bytes 10485760 | tf_op jit(solution)/shard_map/dot_general | solution.py:99
  87.1 0.0 copy-start.1
  87.1 0.0 reduce-scatter.2.cloned.1.call-update
  87.2 1.2 copy-done.1
  88.4 1.5 collective-permute-start
  90.0 0.8 collective-permute-done
  90.8 0.2 maximum_convert_fusion
  91.0 0.6 fusion.27
  91.7 0.6 fusion.30
  92.3 0.4 fusion.3
  92.7 0.0 copy-start.4
  92.8 0.0 copy-done
  92.8 0.5 fusion.24
  93.3 0.2 copy-done.4
  93.4 0.2 fusion.7
  93.6 0.0 copy-start.2
  93.7 22.0 %all-gather.3.cloned.1.call-done = bf16[1024,2048]{1,0:T(8,128)(2,1)} async-done(((bf16[128,2048]{1,0:T(8,128)(2,1)}), bf16[1024,2048]{1,0:T(8,128)(2,1)}) %all-gather.3.cloned.1.call-update) | async-done | bytes 4194320 | tf_op jit(solution)/shard_map/all_gather | solution.py:79
  115.6 4.7 %multiply_reduce_fusion = (f32[512]{0:T(512)S(1)}, f32[512,2048]{1,0:T(8,128)S(1)}) fusion(bf16[512,1024]{0,1:T(8,128)(2,1)S(1)} %fusion.7, bf16[1024,2048]{1,0:T(8,128)(2,1)} %all-gather.3.cloned.1.call-done), kind=kOutput, calls=%fused_computation.1 | convolution fusion | flops 2149580288 | bytes 9439232 | tf_op jit(solution)/shard_map/dot_general | solution.py:77
  120.3 0.0 copy-done.2
  120.3 0.0 copy-start.3
  120.3 1.7 multiply_convert_fusion
  122.1 138.4 %reduce-scatter.2.cloned.1.call-done = bf16[32,2048]{1,0:T(8,128)(2,1)} async-done(((bf16[1024,2048]{1,0:T(8,128)(2,1)}), bf16[32,2048]{1,0:T(8,128)(2,1)}) %reduce-scatter.2.cloned.1.call-update) | async-done | bytes 131088 | tf_op jit(solution)/shard_map/reduce_scatter | solution.py:102
  260.5 1.0 fusion.31
  261.5 0.0 copy-done.3
  261.6 1.7 fusion.33
  (8 shorter events, 0.1 us)
Async XLA Ops:
  7.2 85.6 %copy-start = (bf16[4,256,256]{2,1,0:T(8,128)(2,1)S(1)}, bf16[4,256,256]{2,1,0:T(8,128)(2,1)}, u32[]{:S(2)}) copy-start(bf16[4,256,256]{2,1,0:T(8,128)(2,1)} %param.14) | copy-start | bytes 1572868
  7.2 59.6 %all-gather.5.cloned.1.call-start = ((), (), s32[]{:S(2)}) async-start(), calls=%async_computation.2 | async-start | bytes 5242880 | tf_op jit(solution)/shard_map/all_gather | solution.py:90
  8.8 3.4 %copy-start.5 = (f32[256,4]{0,1:T(4,128)S(1)}, f32[256,4]{0,1:T(4,128)}, u32[]{:S(2)}) copy-start(f32[256,4]{0,1:T(4,128)} %param.20) | copy-start | bytes 12292
  8.8 3.4 %copy-start.6 = (s32[256,4]{0,1:T(4,128)S(1)}, s32[256,4]{0,1:T(4,128)}, u32[]{:S(2)}) copy-start(s32[256,4]{0,1:T(4,128)} %param.19) | copy-start | bytes 12292
  11.3 104.3 %all-gather.3.cloned.1.call-start = ((), (), s32[]{:S(2)}) async-start(), calls=%async_computation.1 | async-start | bytes 4718592 | tf_op jit(solution)/shard_map/all_gather | solution.py:79
  12.1 248.4 %reduce-scatter.2.cloned.1.call-start = ((), (), s32[]{:S(2)}) async-start(), calls=%async_computation.3 | async-start | bytes 4325376 | tf_op jit(solution)/shard_map/reduce_scatter | solution.py:102
  66.8 5.4 %copy-start.7 = (bf16[2,2048,512]{2,1,0:T(8,128)(2,1)S(1)}, bf16[2,2048,512]{2,1,0:T(8,128)(2,1)}, u32[]{:S(2)}) copy-start(bf16[2,2048,512]{2,1,0:T(8,128)(2,1)} %param.23) | copy-start | bytes 12582916
  66.8 5.4 %copy-start.10 = (bf16[1024,2048]{1,0:T(8,128)(2,1)S(1)}, bf16[1024,2048]{1,0:T(8,128)(2,1)}, u32[]{:S(2)}) copy-start(bf16[1024,2048]{1,0:T(8,128)(2,1)} %all-gather.5.cloned.1.call-done) | copy-start | bytes 12582916
  72.2 2.4 copy-start.8
  77.6 3.0 %copy-start.9 = (bf16[2,512,2048]{2,1,0:T(8,128)(2,1)S(1)}, bf16[2,512,2048]{2,1,0:T(8,128)(2,1)}, u32[]{:S(2)}) copy-start(bf16[2,512,2048]{2,1,0:T(8,128)(2,1)} %param.24) | copy-start | bytes 12582916
  87.1 1.3 copy-start.1
  88.4 2.4 collective-permute-start
  92.7 0.7 copy-start.4
  93.6 26.7 %copy-start.2 = (f32[2048]{0:T(1024)S(1)}, f32[2048]{0:T(1024)}, u32[]{:S(2)}) copy-start(f32[2048]{0:T(1024)} %param.17) | copy-start | bytes 24580
  120.3 141.2 %copy-start.3 = (f32[2048]{0:T(1024)S(1)}, f32[2048]{0:T(1024)}, u32[]{:S(2)}) copy-start(f32[2048]{0:T(1024)} %param.25) | copy-start | bytes 24580
Sparse Core Ops, SparseCore 0:
  11.5 55.2 all-gather.4
  68.4 47.2 all-gather.2
  117.9 142.5 reduce-scatter.1

commit v2 on v1

--- a/solution.py
+++ b/solution.py
@@ -1,12 +1,19 @@
+import functools
+
 import jax
 import jax.numpy as jnp
 from jax import lax
+from jax.experimental import pallas as pl
+from jax.experimental.pallas import tpu as pltpu
 from jax.sharding import PartitionSpec as P
 
 WINDOWS = (2, 4, 8, 16)
 EPS = 1e-06
 LIMIT = 7.0
 ALPHA = 1.702
+LANES = 128
+TILE = 512
+MESH = pl.DeviceIdType.MESH
 
 
 def shifted(block, axis, distance):
@@ -44,6 +51,265 @@
     gate = jnp.minimum(gate, LIMIT)
     up = jnp.clip(up, -LIMIT, LIMIT)
     return (up + 1.0) * gate * jax.nn.sigmoid(ALPHA * gate)
+
+
+def flipped(place, mask, count):
+    result, bit = 0, 1
+    while bit < count:
+        result = result + ((place // bit + mask // bit) % 2) * bit
+        bit *= 2
+    return result
+
+
+def expert_kernel(
+    n_ep,
+    n_tp,
+    own_ref,
+    gate_hbm,
+    up_hbm,
+    down_hbm,
+    gain_ref,
+    out_ref,
+    x_ref,
+    gate_ref,
+    up_ref,
+    down_ref,
+    hid_ref,
+    part_ref,
+    core_ref,
+    peer_ref,
+    acc_ref,
+    zsend_ref,
+    zrecv_ref,
+    load_sem,
+    ag_send,
+    ag_recv,
+    fw_send,
+    fw_recv,
+    cs_send,
+    cs_recv,
+    ep_send,
+    ep_recv,
+    z_send,
+    z_recv,
+):
+    ep, tp = lax.axis_index("ep"), lax.axis_index("tp")
+    core, z = tp % 2, tp // 2
+    partner = z * 2 + 1 - core
+    n_z = n_tp // 2
+    tokens = own_ref.shape[0]
+    experts, width, units = gate_ref.shape
+    tiles = width // TILE
+    half = pl.ds(pl.multiple_of(core * (tokens // 2), tokens // 2), tokens // 2)
+    last = n_ep - 1
+
+    loads = [
+        pltpu.make_async_copy(gate_hbm, gate_ref, load_sem.at[0]),
+        pltpu.make_async_copy(up_hbm, up_ref, load_sem.at[1]),
+        pltpu.make_async_copy(down_hbm, down_ref, load_sem.at[2]),
+    ]
+    for load in loads:
+        load.start()
+
+    def ep_peer(k):
+        return {"ep": flipped(ep, k + 1, n_ep)}
+
+    def z_peer(k):
+        return flipped(z, k + 1, n_z)
+
+    barrier = pltpu.get_barrier_semaphore()
+    pl.semaphore_signal(barrier, inc=1, device_id={"tp": partner}, device_id_type=MESH)
+    for k in range(n_ep - 1):
+        pl.semaphore_signal(barrier, inc=1, device_id=ep_peer(k), device_id_type=MESH)
+    for k in range(n_z - 1):
+        pl.semaphore_signal(
+            barrier, inc=1, device_id={"tp": z_peer(k) * 2 + core}, device_id_type=MESH
+        )
+    pl.semaphore_wait(barrier, n_ep + n_z - 1)
+
+    def gather_copy(k):
+        return pltpu.make_async_remote_copy(
+            own_ref.at[half],
+            x_ref.at[k, half],
+            ag_send.at[k],
+            ag_recv.at[k],
+            device_id=ep_peer(k),
+            device_id_type=MESH,
+        )
+
+    def forward_copy(k):
+        return pltpu.make_async_remote_copy(
+            x_ref.at[k, half],
+            x_ref.at[k, half],
+            fw_send.at[k],
+            fw_recv.at[k],
+            device_id={"tp": partner},
+            device_id_type=MESH,
+        )
+
+    def core_copy(k, j):
+        return pltpu.make_async_remote_copy(
+            part_ref.at[j, :, 1 - core],
+            core_ref.at[k, j],
+            cs_send.at[j],
+            cs_recv.at[k, j],
+            device_id={"tp": partner},
+            device_id_type=MESH,
+        )
+
+    def peer_copy(k):
+        return pltpu.make_async_remote_copy(
+            core_ref.at[k],
+            peer_ref.at[k],
+            ep_send.at[k],
+            ep_recv.at[k],
+            device_id=ep_peer(k),
+            device_id_type=MESH,
+        )
+
+    def z_copy(k):
+        return pltpu.make_async_remote_copy(
+            zsend_ref.at[z_peer(k)],
+            zrecv_ref.at[k],
+            z_send.at[k],
+            z_recv.at[k],
+            device_id={"tp": z_peer(k) * 2 + core},
+            device_id_type=MESH,
+        )
+
+    for k in range(n_ep - 1):
+        gather_copy(k).start()
+
+    def compute(k, rows):
+        lane = lax.broadcasted_iota(jnp.int32, (tokens, LANES), 1) % (LANES // 2)
+        packed = rows[:, width:].astype(jnp.float32)
+
+        @pl.loop(0, experts)
+        def _(which):
+            weight = jnp.sum(
+                jnp.where(lane == ep * experts + which, packed, 0.0), axis=1, keepdims=True
+            )
+            values = rows[:, :width]
+            gate = jnp.dot(values, gate_ref[which], preferred_element_type=jnp.float32)
+            up = jnp.dot(values, up_ref[which], preferred_element_type=jnp.float32)
+            hid_ref[which] = (clamped_unit(gate, up) * weight).astype(jnp.bfloat16)
+
+        @pl.loop(0, tiles)
+        def _(j):
+            columns = pl.ds(pl.multiple_of(j * TILE, TILE), TILE)
+            total = jnp.dot(
+                hid_ref[0], down_ref[0, :, columns], preferred_element_type=jnp.float32
+            )
+            for which in range(1, experts):
+                total = total + jnp.dot(
+                    hid_ref[which], down_ref[which, :, columns], preferred_element_type=jnp.float32
+                )
+            part_ref[j] = total.astype(jnp.bfloat16).reshape(part_ref.shape[1:])
+            core_copy(k, j).start()
+
+    for load in loads:
+        load.wait()
+    compute(last, own_ref)
+
+    @pl.loop(0, tiles)
+    def _(j):
+        core_copy(last, j).wait()
+        acc_ref[j] = part_ref[j, :, core].astype(jnp.float32) + core_ref[last, j].astype(
+            jnp.float32
+        )
+
+    @pl.loop(0, n_ep - 1)
+    def _(k):
+        gather_copy(k).wait_recv()
+        forward_copy(k).start()
+        forward_copy(k).wait_recv()
+        compute(k, x_ref.at[k])
+
+        @pl.loop(0, tiles)
+        def _(j):
+            core_copy(k, j).wait()
+            core_ref[k, j] = (
+                part_ref[j, :, core].astype(jnp.float32) + core_ref[k, j].astype(jnp.float32)
+            ).astype(jnp.bfloat16)
+
+        peer_copy(k).start()
+
+    @pl.loop(0, n_ep - 1)
+    def _(k):
+        peer_copy(k).wait_recv()
+        acc_ref[...] += peer_ref[k].astype(jnp.float32)
+
+    for place in range(n_z):
+        zsend_ref[place] = acc_ref[:, place].astype(jnp.bfloat16)
+    for k in range(n_z - 1):
+        z_copy(k).start()
+    total = acc_ref[:, z]
+    for k in range(n_z - 1):
+        z_copy(k).wait_recv()
+        total = total + zrecv_ref[k].astype(jnp.float32)
+    squares = jnp.sum(jnp.sum(total * total, axis=0), axis=-1, keepdims=True)
+    scale = lax.rsqrt(squares / width + EPS)
+    for j in range(tiles):
+        columns = slice(j * TILE, (j + 1) * TILE)
+        out_ref[:, columns] = (total[j] * scale * gain_ref[:, columns]).astype(jnp.bfloat16)
+
+    @pl.loop(0, n_ep - 1)
+    def _(k):
+        gather_copy(k).wait_send()
+        forward_copy(k).wait_send()
+        peer_copy(k).wait_send()
+
+    for k in range(n_z - 1):
+        z_copy(k).wait_send()
+
+
+def experts_mixed(own, gate_weight, up_weight, down_weight, gain, n_ep, n_tp):
+    tokens, wide = own.shape
+    experts, width, units = gate_weight.shape
+    tiles, n_z, block = width // TILE, n_tp // 2, tokens // n_tp
+    dma = pltpu.SemaphoreType.DMA
+    vmem = pl.BlockSpec(memory_space=pltpu.VMEM)
+    hbm = pl.BlockSpec(memory_space=pl.ANY)
+    bf16 = jnp.bfloat16
+    return pl.pallas_call(
+        functools.partial(expert_kernel, n_ep, n_tp),
+        out_shape=jax.ShapeDtypeStruct((block, width), bf16),
+        in_specs=[vmem, hbm, hbm, hbm, vmem],
+        out_specs=vmem,
+        scratch_shapes=[
+            pltpu.VMEM((n_ep - 1, tokens, wide), bf16),
+            pltpu.VMEM(gate_weight.shape, bf16),
+            pltpu.VMEM(up_weight.shape, bf16),
+            pltpu.VMEM(down_weight.shape, bf16),
+            pltpu.VMEM((experts, tokens, units), bf16),
+            pltpu.VMEM((tiles, n_z, 2, block, TILE), bf16),
+            pltpu.VMEM((n_ep, tiles, n_z, block, TILE), bf16),
+            pltpu.VMEM((n_ep - 1, tiles, n_z, block, TILE), bf16),
+            pltpu.VMEM((tiles, n_z, block, TILE), jnp.float32),
+            pltpu.VMEM((n_z, tiles, block, TILE), bf16),
+            pltpu.VMEM((n_z - 1, tiles, block, TILE), bf16),
+            dma((3,)),
+            dma((n_ep - 1,)),
+            dma((n_ep - 1,)),
+            dma((n_ep - 1,)),
+            dma((n_ep - 1,)),
+            dma((tiles,)),
+            dma((n_ep, tiles)),
+            dma((n_ep - 1,)),
+            dma((n_ep - 1,)),
+            dma((n_z - 1,)),
+            dma((n_z - 1,)),
+        ],
+        compiler_params=pltpu.CompilerParams(
+            collective_id=0, has_side_effects=True, vmem_limit_bytes=60 * 2**20
+        ),
+        cost_estimate=pl.CostEstimate(
+            flops=6 * n_ep * tokens * experts * units * width,
+            bytes_accessed=64 * 2**20,
+            transcendentals=0,
+        ),
+        name="experts",
+    )(own, gate_weight, up_weight, down_weight, gain)
 
 
 def body(
@@ -80,29 +346,18 @@
         preferred_element_type=jnp.float32,
     )
     mix_out = rms_scale(projected, mix_gain).astype(jnp.bfloat16)
-    ep_place = lax.axis_index("ep")
-    local_experts = gate_weight.shape[0]
-    experts = local_experts * lax.axis_size("ep")
+    n_ep, n_tp = lax.axis_size("ep"), lax.axis_size("tp")
+    experts = gate_weight.shape[0] * n_ep
     weights = expert_weights(routes, route_weight, experts)
-    weights = lax.all_gather(weights, "ep", axis=0, tiled=True)
-    weights = lax.dynamic_slice_in_dim(weights, ep_place * local_experts, local_experts, 1)
-    normed = rms_scale(expert_in.astype(jnp.float32), pre_gain).astype(jnp.bfloat16)
-    normed = lax.all_gather(normed, "ep", axis=0, tiled=True)
-    hidden = []
-    for which in range(local_experts):
-        gate = jnp.dot(normed, gate_weight[which], preferred_element_type=jnp.float32)
-        up = jnp.dot(normed, up_weight[which], preferred_element_type=jnp.float32)
-        hidden.append(
-            (clamped_unit(gate, up) * weights[:, which : which + 1]).astype(jnp.bfloat16)
-        )
-    hidden = jnp.concatenate(hidden, axis=1)
-    partial = jnp.dot(
-        hidden, down_weight.reshape(-1, width), preferred_element_type=jnp.float32
+    high = lax.reduce_precision(weights, 8, 7)
+    fill = ((0, 0), (0, LANES // 2 - experts))
+    normed = rms_scale(expert_in.astype(jnp.float32), pre_gain)
+    own = jnp.concatenate(
+        [normed, jnp.pad(high, fill), jnp.pad(weights - high, fill)], axis=1
     ).astype(jnp.bfloat16)
-    combined = lax.psum_scatter(
-        partial, ("ep", "tp"), scatter_dimension=0, tiled=True
-    ).astype(jnp.float32)
-    expert_out = rms_scale(combined, post_gain).astype(jnp.bfloat16)
+    expert_out = experts_mixed(
+        own, gate_weight, up_weight, down_weight, post_gain[None, :], n_ep, n_tp
+    )
     return (mix_out, expert_out)
 
 

time: 270 us -> 104 us (0.39)
  waiting for transfers between devices: 207 us -> 0.7 us
  Pallas kernels: 0 us -> 72.5 us
  matrix products: 25.4 us -> 5.14 us
  blocking collectives: 9.67 us -> 0 us
  other arithmetic: 10.7 us -> 5.21 us
    reduce_scatter x1 -> x0, waiting for transfers between devices: 138 us -> none  [body(): lax.psum_scatter(partial, ('ep', 'tp'), scatter_dimension=0, tiled=True)]
    pallas_call x0 -> x1, Pallas kernels: none -> 72.5 us  [experts_mixed(): pl.pallas_call(functools.partial(expert_kernel, n_ep, n_tp), out_shape=ja...]
    all_gather x1 -> x0, waiting for transfers between devices: 44.9 us -> none  [body(): normed = lax.all_gather(normed, 'ep', axis=0, tiled=True)]
    all_gather x1, waiting for transfers between devices: 22 us -> 0.02 us  [body(): lax.all_gather(out_weight, 'tp', axis=0, tiled=True)]
    dot_general x5 -> x0, matrix products: 20.2 us -> none  [the longest x2 7.79 us: body(): up = jnp.dot(normed, up_weight[which], preferred_element_type=jnp.float32)]
    all_gather x1 -> x0, blocking collectives: 9.67 us -> none  [body(): weights = lax.all_gather(weights, 'ep', axis=0, tiled=True)]
    convert_element_type x2 -> x0, other arithmetic: 4.16 us -> none  [the longest x1 2.5 us: body(): rms_scale(expert_in.astype(jnp.float32), pre_gain).astype(jnp.bfloat16)]
  transfers between devices with their start and end apart: 4 -> 2, of which waited for: 4 -> 0; matrix products, arithmetic and copies ran while one was open for 11% -> 7% of each run, Pallas kernels for 0% -> 70%
where the time goes in v2:
time: 104 us
  Pallas kernels  72.5 us (70%)
  between operations  14.3 us (14%)
  other arithmetic  5.21 us (5%)
  matrix products  5.14 us (5%)
  local copies, waits for them, and re-layouts  3.76 us (4%)
  starting transfers between devices  2.42 us (2%)
    pallas_call x1, Pallas kernels, experts_mixed(): pl.pallas_call(functools.partial(expert_kernel, n_ep, n_tp), out_shape=ja...  72.5 us
    dot_general x1, matrix products, body(): jnp.dot(mixed, lax.all_gather(out_weight, 'tp', axis=0, tiled=True), pref...  4.66 us
    ppermute x1, starting transfers between devices, shifted(): return lax.ppermute(block, axis, route)  2.39 us
  transfers between devices with their start and end apart: 2, of which 0 were waited for; matrix products, arithmetic and copies ran while one was open for 7% of the time, Pallas kernels for 70%

profile of v2, /device:TPU:0, one launch (start us, length us, event | category | flops | bytes accessed | tf_op | source)
XLA Modules:
  0.0 104.0 jit_solution(13029830745666699174)
XLA Ops:
  7.2 0.0 copy-start
  7.2 0.0 copy-start.1
  7.2 0.0 copy-start.4
  7.2 0.0 all-gather.2.cloned.1.call-start
  7.2 0.7 all-gather.2.cloned.1.call-update
  7.9 0.8 slice.130
  8.7 2.4 %collective-permute-start = (bf16[16,1024]{1,0:T(8,128)(2,1)S(1)}, bf16[16,1024]{1,0:T(8,128)(2,1)S(1)}, u32[]{:S(2)}, u32[]{:S(2)}) collective-permute-start(bf16[16,1024]{1,0:T(8,128)(2,1)S(1)} %slice.130), channel_id=1, source_target_pairs={{0,1},{1,2},{2,3},{3,4},{4,5},{5,6},{6,7},{7,8},{8,9},{9,10},{10,1... | collective-permute-start | bytes 98312 | tf_op jit(solution)/shard_map/ppermute | solution.py:22
  11.1 0.7 select_reduce_fusion
  11.8 0.1 copy.26
  12.0 0.1 copy.25
  12.2 0.0 copy-done.1
  12.2 0.3 fusion
  12.5 0.0 copy-done.4
  12.5 0.3 fusion.2
  12.8 1.9 %concatenate.12.own_ref = bf16[256,2176]{1,0:T(8,128)(2,1)} concatenate(bf16[256,2048]{1,0:T(8,128)(2,1)S(1)} %fusion.2, bf16[256,64]{1,0:T(8,128)(2,1)S(1)} %pad.9, bf16[256,64]{1,0:T(8,128)(2,1)S(1)} %pad.10), dimensions={1} | concatenate | bytes 2228224 | tf_op jit(solution)/shard_map/concatenate | solution.py:355
  14.7 0.0 copy-start.2
  14.7 72.5 %experts.1 = bf16[32,2048]{1,0:T(8,128)(2,1)} custom-call(bf16[256,2176]{1,0:T(8,128)(2,1)} %concatenate.12.own_ref, bf16[2,2048,512]{2,1,0:T(8,128)(2,1)} %gate_hbm.1, bf16[2,2048,512]{2,1,0:T(8,128)(2,1)} %up_hbm.1, bf16[2,512,2048]{2,1,0:T(8,128)(2,1)} %down_hbm.1, f32[1,2048]{1,0:T(1,128)} %bitcast.15), custom_call_target="tpu_custom_call" | custom-call | flops 12884901888 | bytes 67108864 | tf_op jit(solution)/shard_map/experts/pallas_call | solution.py:274
  87.1 0.0 collective-permute-done
  87.1 0.0 copy-done.2
  87.2 0.2 maximum_convert_fusion
  87.4 0.6 fusion.8
  88.0 0.6 fusion.11
  88.7 0.4 fusion.3
  89.1 0.0 copy-start.6
  89.1 0.0 copy-done
  89.1 0.5 fusion.5
  89.6 0.2 copy-done.6
  89.8 0.2 fusion.4
  90.0 0.0 copy-start.5
  90.0 0.0 all-gather.2.cloned.1.call-done
  90.0 4.7 %multiply_reduce_fusion = (f32[512]{0:T(512)S(1)}, f32[512,2048]{1,0:T(8,128)S(1)}) fusion(bf16[512,1024]{0,1:T(8,128)(2,1)S(1)} %fusion.4, bf16[1024,2048]{1,0:T(8,128)(2,1)} %all-gather.2.cloned.1.call-done), kind=kOutput, calls=%fused_computation.1 | convolution fusion | flops 2149580288 | bytes 9439232 | tf_op jit(solution)/shard_map/dot_general | solution.py:343
  94.7 0.0 copy-done.5
  94.7 0.0 copy-start.3
  94.7 1.7 %multiply_convert_fusion = bf16[512,2048]{1,0:T(8,128)(2,1)} fusion(f32[512,2048]{1,0:T(8,128)S(1)} %get-tuple-element.8, f32[2048]{0:T(1024)S(1)} %copy-done.5, f32[512]{0:T(512)S(1)} %add_rsqrt_fusion), kind=kLoop, calls=%fused_computation | loop fusion | flops 3145728 | bytes 6301696 | tf_op jit(solution)/shard_map/convert_element_type | solution.py:348
  96.4 0.0 copy-done.3
  96.5 0.7 copy.35
  (8 shorter events, 0.1 us)
Async XLA Ops:
  7.2 81.9 %copy-start = (bf16[4,256,256]{2,1,0:T(8,128)(2,1)S(1)}, bf16[4,256,256]{2,1,0:T(8,128)(2,1)}, u32[]{:S(2)}) copy-start(bf16[4,256,256]{2,1,0:T(8,128)(2,1)} %param.14) | copy-start | bytes 1572868
  7.2 5.0 %copy-start.1 = (bf16[256,2048]{1,0:T(8,128)(2,1)S(1)}, bf16[256,2048]{1,0:T(8,128)(2,1)}, u32[]{:S(2)}) copy-start(bf16[256,2048]{1,0:T(8,128)(2,1)} %param.18) | copy-start | bytes 3145732
  7.2 5.3 %copy-start.4 = (f32[2048]{0:T(1024)S(1)}, f32[2048]{0:T(1024)}, u32[]{:S(2)}) copy-start(f32[2048]{0:T(1024)} %param.21) | copy-start | bytes 24580
  7.2 82.8 %all-gather.2.cloned.1.call-start = ((), (), s32[]{:S(2)}) async-start(), calls=%async_computation | async-start | bytes 4718592 | tf_op jit(solution)/shard_map/all_gather | solution.py:345
  8.7 78.4 %collective-permute-start = (bf16[16,1024]{1,0:T(8,128)(2,1)S(1)}, bf16[16,1024]{1,0:T(8,128)(2,1)S(1)}, u32[]{:S(2)}, u32[]{:S(2)}) collective-permute-start(bf16[16,1024]{1,0:T(8,128)(2,1)S(1)} %slice.130), channel_id=1, source_target_pairs={{0,1},{1,2},{2,3},{3,4},{4,5},{5,6},{6,7},{7,8},{8,9},{9,10},{10,1... | collective-permute-start | bytes 98312 | tf_op jit(solution)/shard_map/ppermute | solution.py:22
  14.7 72.5 %copy-start.2 = (bf16[512,1024]{1,0:T(8,128)(2,1)S(1)}, bf16[512,1024]{1,0:T(8,128)(2,1)}, u32[]{:S(2)}) copy-start(bf16[512,1024]{1,0:T(8,128)(2,1)} %param.13) | copy-start | bytes 3145732
  89.1 0.7 copy-start.6
  90.0 4.7 %copy-start.5 = (f32[2048]{0:T(1024)S(1)}, f32[2048]{0:T(1024)}, u32[]{:S(2)}) copy-start(f32[2048]{0:T(1024)} %param.17) | copy-start | bytes 24580
  94.7 1.7 %copy-start.3 = (bf16[32,2048]{1,0:T(8,128)(2,1)S(1)}, bf16[32,2048]{1,0:T(8,128)(2,1)}, u32[]{:S(2)}) copy-start(bf16[32,2048]{1,0:T(8,128)(2,1)} %experts.1) | copy-start | bytes 393220
Sparse Core Ops, SparseCore 0:
  9.6 49.5 all-gather.1

commit v3 on v2

--- a/solution.py
+++ b/solution.py
@@ -13,33 +13,14 @@
 ALPHA = 1.702
 LANES = 128
 TILE = 512
+POOL_ROWS = 128
+PROJECT_ROWS = 256
 MESH = pl.DeviceIdType.MESH
-
-
-def shifted(block, axis, distance):
-    devices = range(lax.axis_size(axis))
-    route = [(i - distance, i) for i in devices if i - distance in devices]
-    return lax.ppermute(block, axis, route)
 
 
 def rms_scale(values, gain):
     mean_square = jnp.mean(values * values, axis=-1, keepdims=True)
     return values * lax.rsqrt(mean_square + EPS) * gain
-
-
-def trailing_pool(padded, first_pos, rows):
-    group = padded.shape[1] // 4
-    position = first_pos + jnp.arange(rows, dtype=jnp.int32)
-    pieces = []
-    for which, window in enumerate(WINDOWS):
-        channels = padded[:, which * group : (which + 1) * group]
-        running = channels[16 : 16 + rows]
-        for reach in range(2, window + 1):
-            running = running + channels[17 - reach : 17 - reach + rows]
-        count = jnp.minimum(position + 1, window).astype(jnp.float32)[:, None]
-        pieces.append(running / count)
-    pooled = jnp.concatenate(pieces, axis=1)
-    return (pooled - padded[16:]).astype(jnp.bfloat16)
 
 
 def expert_weights(routes, route_weight, experts):
@@ -64,12 +45,25 @@
 def expert_kernel(
     n_ep,
     n_tp,
-    own_ref,
+    expert_in_ref,
+    packed_ref,
+    pre_gain_ref,
     gate_hbm,
     up_hbm,
     down_hbm,
     gain_ref,
+    pool_ref,
+    pool_weight_ref,
+    pool_gain_ref,
+    out_weight_ref,
+    mix_gain_ref,
+    mix_ref,
     out_ref,
+    own_ref,
+    rim_ref,
+    padded_ref,
+    mixed_ref,
+    all_weight_ref,
     x_ref,
     gate_ref,
     up_ref,
@@ -92,6 +86,12 @@
     ep_recv,
     z_send,
     z_recv,
+    rim_send,
+    rim_recv,
+    w_send,
+    w_recv,
+    wf_send,
+    wf_recv,
 ):
     ep, tp = lax.axis_index("ep"), lax.axis_index("tp")
     core, z = tp % 2, tp // 2
@@ -117,7 +117,16 @@
     def z_peer(k):
         return flipped(z, k + 1, n_z)
 
+    place = ep * n_tp + tp
+    devices = n_ep * n_tp
+    after, before = (place + 1) % devices, (place + devices - 1) % devices
+
+    def at(device):
+        return {"ep": device // n_tp, "tp": device % n_tp}
+
     barrier = pltpu.get_barrier_semaphore()
+    pl.semaphore_signal(barrier, inc=1, device_id=at(after), device_id_type=MESH)
+    pl.semaphore_signal(barrier, inc=1, device_id=at(before), device_id_type=MESH)
     pl.semaphore_signal(barrier, inc=1, device_id={"tp": partner}, device_id_type=MESH)
     for k in range(n_ep - 1):
         pl.semaphore_signal(barrier, inc=1, device_id=ep_peer(k), device_id_type=MESH)
@@ -125,7 +134,11 @@
         pl.semaphore_signal(
             barrier, inc=1, device_id={"tp": z_peer(k) * 2 + core}, device_id_type=MESH
         )
-    pl.semaphore_wait(barrier, n_ep + n_z - 1)
+    own_ref[:, :width] = rms_scale(
+        expert_in_ref[...].astype(jnp.float32), pre_gain_ref[...]
+    ).astype(jnp.bfloat16)
+    own_ref[:, width:] = packed_ref[...]
+    pl.semaphore_wait(barrier, n_ep + n_z + 1)
 
     def gather_copy(k):
         return pltpu.make_async_remote_copy(
@@ -177,8 +190,108 @@
             device_id_type=MESH,
         )
 
+    rows, channels = pool_ref.shape
+    rim_copy = pltpu.make_async_remote_copy(
+        pool_ref.at[pl.ds(rows - 16, 16)],
+        rim_ref,
+        rim_send,
+        rim_recv,
+        device_id=at(after),
+        device_id_type=MESH,
+    )
+
+    def weight_copy(k):
+        return pltpu.make_async_remote_copy(
+            out_weight_ref,
+            all_weight_ref.at[tp],
+            w_send.at[k],
+            w_recv.at[k],
+            device_id={"tp": z_peer(k) * 2 + core},
+            device_id_type=MESH,
+        )
+
+    def weight_forward(k):
+        if k == n_z - 1:
+            source, target = out_weight_ref, all_weight_ref.at[tp]
+        else:
+            target = all_weight_ref.at[z_peer(k) * 2 + core]
+            source = target
+        return pltpu.make_async_remote_copy(
+            source,
+            target,
+            wf_send.at[k],
+            wf_recv.at[k],
+            device_id={"tp": partner},
+            device_id_type=MESH,
+        )
+
     for k in range(n_ep - 1):
         gather_copy(k).start()
+    rim_copy.start()
+    for k in range(n_z - 1):
+        weight_copy(k).start()
+    weight_forward(n_z - 1).start()
+
+    def pool():
+        padded_ref[: POOL_ROWS - 16] = jnp.zeros((POOL_ROWS - 16, channels), jnp.bfloat16)
+        rim_copy.wait_recv()
+
+        @pl.when(place == 0)
+        def _():
+            padded_ref[POOL_ROWS - 16 : POOL_ROWS] = jnp.zeros((16, channels), jnp.bfloat16)
+
+        @pl.when(place != 0)
+        def _():
+            padded_ref[POOL_ROWS - 16 : POOL_ROWS] = rim_ref[...]
+
+        padded_ref[POOL_ROWS:] = pool_ref[...]
+        group = channels // 4
+        reach = (
+            lax.broadcasted_iota(jnp.int32, (POOL_ROWS, 2 * POOL_ROWS), 0)
+            + POOL_ROWS
+            - lax.broadcasted_iota(jnp.int32, (POOL_ROWS, 2 * POOL_ROWS), 1)
+        )
+        local = lax.broadcasted_iota(jnp.int32, (POOL_ROWS, 1), 0)
+
+        @pl.loop(0, rows // POOL_ROWS)
+        def _(i):
+            start = pl.multiple_of(i * POOL_ROWS, POOL_ROWS)
+            here = pl.ds(start, POOL_ROWS)
+            position = place * rows + start + local
+            for which, window in enumerate(WINDOWS):
+                columns = slice(which * group, (which + 1) * group)
+                band = jnp.where((reach >= 0) & (reach < window), 1.0, 0.0).astype(jnp.bfloat16)
+                running = jnp.dot(
+                    band,
+                    padded_ref[pl.ds(start, 2 * POOL_ROWS), columns],
+                    preferred_element_type=jnp.float32,
+                )
+                count = jnp.minimum(position + 1, window).astype(jnp.float32)
+                diff = running / count - pool_ref[here, columns].astype(jnp.float32)
+                mixed = jnp.dot(
+                    diff.astype(jnp.bfloat16),
+                    pool_weight_ref[which],
+                    preferred_element_type=jnp.float32,
+                )
+                mixed_ref[here, columns] = (mixed * pool_gain_ref[:, columns]).astype(jnp.bfloat16)
+
+    def project():
+        all_weight_ref[tp] = out_weight_ref[...]
+        for k in range(n_z - 1):
+            weight_copy(k).wait_recv()
+            weight_forward(k).start()
+        for k in range(n_z):
+            weight_forward(k).wait_recv()
+
+        @pl.loop(0, rows // PROJECT_ROWS)
+        def _(i):
+            here = pl.ds(pl.multiple_of(i * PROJECT_ROWS, PROJECT_ROWS), PROJECT_ROWS)
+            projected = jnp.dot(
+                mixed_ref[here],
+                all_weight_ref[...].reshape(channels, width),
+                preferred_element_type=jnp.float32,
+            )
+            mix_ref[here] = rms_scale(projected, mix_gain_ref[...]).astype(jnp.bfloat16)
 
     def compute(k, rows):
         lane = lax.broadcasted_iota(jnp.int32, (tokens, LANES), 1) % (LANES // 2)
@@ -218,6 +331,8 @@
             jnp.float32
         )
 
+    pool()
+
     @pl.loop(0, n_ep - 1)
     def _(k):
         gather_copy(k).wait_recv()
@@ -234,13 +349,15 @@
 
         peer_copy(k).start()
 
+    project()
+
     @pl.loop(0, n_ep - 1)
     def _(k):
         peer_copy(k).wait_recv()
         acc_ref[...] += peer_ref[k].astype(jnp.float32)
 
-    for place in range(n_z):
-        zsend_ref[place] = acc_ref[:, place].astype(jnp.bfloat16)
+    for spot in range(n_z):
+        zsend_ref[spot] = acc_ref[:, spot].astype(jnp.bfloat16)
     for k in range(n_z - 1):
         z_copy(k).start()
     total = acc_ref[:, z]
@@ -261,10 +378,17 @@
 
     for k in range(n_z - 1):
         z_copy(k).wait_send()
-
-
-def experts_mixed(own, gate_weight, up_weight, down_weight, gain, n_ep, n_tp):
-    tokens, wide = own.shape
+        weight_copy(k).wait_send()
+    for k in range(n_z):
+        weight_forward(k).wait_send()
+    rim_copy.wait_send()
+
+
+def fused(operands, n_ep, n_tp):
+    expert_in, packed, _, gate_weight, up_weight, down_weight = operands[:6]
+    pool_in, out_weight = operands[7], operands[10]
+    tokens, wide = expert_in.shape[0], expert_in.shape[1] + packed.shape[1]
+    rows, channels = pool_in.shape
     experts, width, units = gate_weight.shape
     tiles, n_z, block = width // TILE, n_tp // 2, tokens // n_tp
     dma = pltpu.SemaphoreType.DMA
@@ -273,10 +397,18 @@
     bf16 = jnp.bfloat16
     return pl.pallas_call(
         functools.partial(expert_kernel, n_ep, n_tp),
-        out_shape=jax.ShapeDtypeStruct((block, width), bf16),
-        in_specs=[vmem, hbm, hbm, hbm, vmem],
-        out_specs=vmem,
+        out_shape=(
+            jax.ShapeDtypeStruct((rows, width), bf16),
+            jax.ShapeDtypeStruct((block, width), bf16),
+        ),
+        in_specs=[vmem] * 3 + [hbm] * 3 + [vmem] * 6,
+        out_specs=(vmem, vmem),
         scratch_shapes=[
+            pltpu.VMEM((tokens, wide), bf16),
+            pltpu.VMEM((16, channels), bf16),
+            pltpu.VMEM((POOL_ROWS + rows, channels), bf16),
+            pltpu.VMEM((rows, channels), bf16),
+            pltpu.VMEM((n_tp,) + out_weight.shape, bf16),
             pltpu.VMEM((n_ep - 1, tokens, wide), bf16),
             pltpu.VMEM(gate_weight.shape, bf16),
             pltpu.VMEM(up_weight.shape, bf16),
@@ -299,9 +431,15 @@
             dma((n_ep - 1,)),
             dma((n_z - 1,)),
             dma((n_z - 1,)),
+            dma,
+            dma,
+            dma((n_z - 1,)),
+            dma((n_z - 1,)),
+            dma((n_z,)),
+            dma((n_z,)),
         ],
         compiler_params=pltpu.CompilerParams(
-            collective_id=0, has_side_effects=True, vmem_limit_bytes=60 * 2**20
+            collective_id=0, has_side_effects=True, vmem_limit_bytes=67043328
         ),
         cost_estimate=pl.CostEstimate(
             flops=6 * n_ep * tokens * experts * units * width,
@@ -309,7 +447,7 @@
             transcendentals=0,
         ),
         name="experts",
-    )(own, gate_weight, up_weight, down_weight, gain)
+    )(*operands)
 
 
 def body(
@@ -327,38 +465,27 @@
     down_weight,
     post_gain,
 ):
-    rows, channels = pool_in.shape
-    width = out_weight.shape[1]
-    rim = shifted(pool_in[rows - 16 :], ("ep", "tp"), 1)
-    padded = jnp.concatenate([rim, pool_in], axis=0).astype(jnp.float32)
-    first_pos = (lax.axis_index("ep") * lax.axis_size("tp") + lax.axis_index("tp")) * rows
-    diff = trailing_pool(padded, first_pos, rows)
-    mixed = jnp.einsum(
-        "sgc,gcd->sgd",
-        diff.reshape(rows, 4, channels // 4),
-        pool_weight,
-        preferred_element_type=jnp.float32,
-    )
-    mixed = (mixed.reshape(rows, channels) * pool_gain).astype(jnp.bfloat16)
-    projected = jnp.dot(
-        mixed,
-        lax.all_gather(out_weight, "tp", axis=0, tiled=True),
-        preferred_element_type=jnp.float32,
-    )
-    mix_out = rms_scale(projected, mix_gain).astype(jnp.bfloat16)
     n_ep, n_tp = lax.axis_size("ep"), lax.axis_size("tp")
     experts = gate_weight.shape[0] * n_ep
     weights = expert_weights(routes, route_weight, experts)
     high = lax.reduce_precision(weights, 8, 7)
     fill = ((0, 0), (0, LANES // 2 - experts))
-    normed = rms_scale(expert_in.astype(jnp.float32), pre_gain)
-    own = jnp.concatenate(
-        [normed, jnp.pad(high, fill), jnp.pad(weights - high, fill)], axis=1
-    ).astype(jnp.bfloat16)
-    expert_out = experts_mixed(
-        own, gate_weight, up_weight, down_weight, post_gain[None, :], n_ep, n_tp
+    packed = jnp.concatenate([jnp.pad(high, fill), jnp.pad(weights - high, fill)], axis=1)
+    operands = (
+        expert_in,
+        packed.astype(jnp.bfloat16),
+        pre_gain[None, :],
+        gate_weight,
+        up_weight,
+        down_weight,
+        post_gain[None, :],
+        pool_in,
+        pool_weight,
+        pool_gain[None, :],
+        out_weight,
+        mix_gain[None, :],
     )
-    return (mix_out, expert_out)
+    return fused(operands, n_ep, n_tp)
 
 
 def solution(mesh):

time: 104 us -> 80.8 us (0.78)
  between operations: 14.3 us -> 0.67 us
  matrix products: 5.14 us -> 0 us
  other arithmetic: 5.21 us -> 1.47 us
  starting transfers between devices: 2.42 us -> 0 us
  Pallas kernels: 72.5 us -> 74.3 us
    dot_general x2 -> x0, matrix products: 5.14 us -> none  [the longest x1 4.66 us: body(): jnp.dot(mixed, lax.all_gather(out_weight, 'tp', axis=0, tiled=True), pref...]
    unnamed x15 -> x4, local copies, waits for them, and re-layouts: 0.87 us -> 3.85 us
    convert_element_type x6 -> x0, other arithmetic: 2.59 us -> none  [the longest x1 1.73 us: body(): mix_out = rms_scale(projected, mix_gain).astype(jnp.bfloat16)]
    ppermute x1 -> x0, starting transfers between devices: 2.39 us -> none  [shifted(): return lax.ppermute(block, axis, route)]
    pallas_call x1, Pallas kernels: 72.5 us -> 74.3 us  [fused(): pl.pallas_call(functools.partial(expert_kernel, n_ep, n_tp), out_shape=(j...]
    concatenate x1 -> x0, local copies, waits for them, and re-layouts: 1.85 us -> none  [body(): jnp.concatenate([normed, jnp.pad(high, fill), jnp.pad(weights - high, fil...]
    div x2 -> x0, other arithmetic: 1.27 us -> none  [trailing_pool(): pieces.append(running / count)]
  transfers between devices with their start and end apart: 2 -> 0, of which waited for: 0 -> 0; matrix products, arithmetic and copies ran while one was open for 7% -> 0% of each run, Pallas kernels for 70% -> 0%
where the time goes in v3:
time: 80.8 us; the launch traced here: 80.6 us
  Pallas kernels  74.3 us (92%)
  local copies, waits for them, and re-layouts  4.1 us (5%)
  other arithmetic  1.47 us (2%)
    pallas_call x1, Pallas kernels, fused(): pl.pallas_call(functools.partial(expert_kernel, n_ep, n_tp), out_shape=(j...  74.3 us
    unnamed x4, local copies, waits for them, and re-layouts  3.85 us

profile of v3, /device:TPU:0, one launch (start us, length us, event | category | flops | bytes accessed | tf_op | source)
XLA Modules:
  0.0 80.6 jit_solution(750679530506710918)
XLA Ops:
  0.6 0.7 select_reduce_fusion
  1.4 0.1 copy.20
  1.5 0.1 copy.19
  1.6 0.7 fusion.2.packed_ref
  2.4 74.3 %experts.1 = (bf16[512,2048]{1,0:T(8,128)(2,1)}, bf16[32,2048]{1,0:T(8,128)(2,1)}) custom-call(bf16[256,2048]{1,0:T(8,128)(2,1)} %expert_in_ref.1, bf16[256,128]{1,0:T(8,128)(2,1)} %fusion.2.packed_ref, f32[1,2048]{1,0:T(1,128)} %bitcast.4, bf16[2,2048,512]{2,1,0:T(8,128)(2,1)} %gate_hbm.1, bf16[2,2048,512]{2,1,0:T(8,128)(2,1)} %up_hbm.1, ...), custom_call_target="tpu_custom_call" | custom-call | flops 12884901888 | bytes 67108864 | tf_op jit(solution)/shard_map/experts/pallas_call | solution.py:398
  76.7 0.0 copy-start
  76.7 3.2 %copy.24 = bf16[512,2048]{1,0:T(8,128)(2,1)} copy(bf16[512,2048]{1,0:T(8,128)(2,1)} %get-tuple-element.6) | data formatting | bytes 4194304
  79.9 0.0 copy-done
  79.9 0.7 copy.25
  (2 shorter events, 0.0 us)
Async XLA Ops:
  76.7 3.2 %copy-start = (bf16[32,2048]{1,0:T(8,128)(2,1)S(1)}, bf16[32,2048]{1,0:T(8,128)(2,1)}, u32[]{:S(2)}) copy-start(bf16[32,2048]{1,0:T(8,128)(2,1)} %get-tuple-element.7) | copy-start | bytes 393220
